TPU v7x, 32 devices: a whole 2x2x4 slice. The times are simulated.
32 devices in a mesh: ep: 8 (over z, y), tp: 4 (over x, core).
Axes of the slice: x: 2, y: 2, z: 4, core: 2. Of those that a mesh axis runs over, the one named last changes fastest.
Arguments:
- tokens: bfloat16 [1024, 2048], P('ep', 'tp'), may hold values from -6 to 6
- norm_gain: bfloat16 [2048], P('tp'), may hold values from 0.099609375 to 1.8984375
- routes: int32 [1024, 2], P('ep'), may hold values from 0 to 7, as said below
- gate_weights: float32 [1024, 2], P('ep'), may hold values from 0.1 to 1
- w_gate: bfloat16 [8, 2048, 4096], P('ep', None, 'tp'), may hold values from -0.125 to 0.125
- w_up: bfloat16 [8, 2048, 4096], P('ep', None, 'tp'), may hold values from -0.125 to 0.125
- w_down: bfloat16 [8, 4096, 2048], P('ep', 'tp'), may hold values from -0.875 to 0.875
- out_gain: bfloat16 [2048], P('tp'), may hold values from 0.099609375 to 1.8984375
Outputs:
- mixed: bfloat16 [1024, 2048], P('ep', 'tp')
Inputs may be any that keep to these rules, and one draw needn't show every extreme that they name: `routes`: each row names 2 different experts of one group (their quotients by 8 agree). In each aligned block of 128 rows no expert is named by more than 64 rows, and in every block some expert is named by exactly 64 rows.
All inputs are finite; a program needn't handle non-finite values.
Results may differ from a plain program's by a relative error of at most 0.019.
Values may be sent and summed in bfloat16 or wider, within the bound.
A program may use at most 64 MiB of HBM per device.

v0:
```python
import jax
import jax.numpy as jnp
from jax import lax
from jax.sharding import PartitionSpec as P

epsilon = 1e-06


def shards(tokens, norm_gain, routes, gate_weights, w_gate, w_up, w_down, out_gain):
    tok_rows = tokens.shape[0]
    width_local = tokens.shape[1]
    full_width = width_local * lax.axis_size("tp")
    experts = lax.axis_size("ep")
    top_count = routes.shape[1]
    capacity = 2 * top_count * tok_rows // experts
    flat_ids = routes.reshape(-1)
    onehot = (flat_ids[:, None] == jnp.arange(experts, dtype=jnp.int32)[None, :]).astype(jnp.int32)
    before = jnp.cumsum(onehot, axis=0) - onehot
    slot_index = jnp.sum(before * onehot, axis=1)
    dest_index = flat_ids * capacity + slot_index
    dest_pairs = dest_index.reshape(tok_rows, top_count)
    places = jnp.arange(experts * capacity, dtype=jnp.int32)
    scatter_mat = jnp.any(dest_pairs[None, :, :] == places[:, None, None], axis=2).astype(
        jnp.bfloat16
    )
    gate_mat = w_gate[0]
    up_mat = w_up[0]
    x_float = tokens.astype(jnp.float32)
    row_sums = lax.psum(jnp.sum(x_float * x_float, axis=1), "tp")
    scale_in = lax.rsqrt(row_sums / full_width + epsilon)
    normed = (x_float * scale_in[:, None] * norm_gain.astype(jnp.float32)).astype(jnp.bfloat16)
    outgoing = jnp.dot(scatter_mat, normed, preferred_element_type=jnp.float32).astype(jnp.bfloat16)
    arrived = lax.all_to_all(outgoing, "ep", split_axis=0, concat_axis=0, tiled=True)
    portion = lax.all_gather(arrived, "tp", axis=1, tiled=True)
    gate_sum = jnp.dot(portion, gate_mat, preferred_element_type=jnp.float32)
    up_sum = jnp.dot(portion, up_mat, preferred_element_type=jnp.float32)
    hidden = (jax.nn.silu(gate_sum) * up_sum).astype(jnp.bfloat16)
    down_mat = w_down[0]
    summed = lax.psum_scatter(
        lax.dot_general(
            down_mat, hidden, (((0,), (1,)), ((), ())), preferred_element_type=jnp.float32
        ).astype(jnp.bfloat16),
        "tp",
        scatter_dimension=0,
        tiled=True,
    )
    came_back = lax.all_to_all(summed, "ep", split_axis=1, concat_axis=1, tiled=True)
    picked = (
        jnp.take(came_back, dest_index, axis=1)
        .astype(jnp.float32)
        .reshape(width_local, tok_rows, top_count)
    )
    combined = jnp.sum(picked * gate_weights[None, :, :], axis=2).T
    out_sums = lax.psum(jnp.sum(combined * combined, axis=1), "tp")
    scale_out = lax.rsqrt(out_sums / full_width + epsilon)
    return (combined * scale_out[:, None] * out_gain.astype(jnp.float32)).astype(jnp.bfloat16)


def solution(mesh):
    placed = (
        P("ep", "tp"),
        P("tp"),
        P("ep", None),
        P("ep", None),
        P("ep", None, "tp"),
        P("ep", None, "tp"),
        P("ep", "tp", None),
        P("tp"),
    )
    return jax.shard_map(
        shards, mesh=mesh, in_specs=placed, out_specs=P("ep", "tp"), check_vma=False
    )
```

profile of v0, /device:TPU:0, one launch (start us, length us, event | category | flops | bytes accessed | tf_op | source)
XLA Modules:
  0.0 145.3 jit_solution(15379768702945613426)
XLA Ops:
  6.5 0.8 copy.21
  7.3 0.1 eq.39
  7.5 0.1 reshape.77
  7.6 0.6 reduce-window.6
  8.2 0.2 slice_reduce_fusion
  8.5 0.1 fusion.25
  8.6 0.1 reduce_sum.41
  8.7 0.1 copy.23
  8.8 0.7 compare_and_fusion
  9.5 0.1 fusion.16
  9.5 0.7 convert_element_type.45
  10.2 1.0 fusion.17
  11.2 8.4 %psum.14 = f32[128]{0:T(128)S(1)} all-reduce(f32[128]{0:T(128)S(1)} %fusion.17), channel_id=1, replica_groups=mesh['ep'=8,'tp'=4] {'tp'}, use_global_device_ids=true, to_apply=%region_5.6 | all-reduce | flops 128 | bytes 1024 | tf_op jit(solution)/shard_map/psum | solution.py:29
  19.6 1.3 convolution_convert_fusion
  20.9 19.0 %all_to_all.24 = bf16[8,64,512]{2,1,0:T(8,128)(2,1)} all-to-all(bf16[8,64,512]{2,1,0:T(8,128)(2,1)S(1)} %bitcast.43), channel_id=1, replica_groups=mesh['ep'=8,'tp'=4] {'ep'}, dimensions={0} | all-to-all | bytes 1048576 | tf_op jit(solution)/shard_map/all_to_all | solution.py:33
  39.9 0.0 reduce-scatter.2.cloned.1.call-start
  40.0 21.8 %all-gather.2.cloned.1.call-done = bf16[512,2048]{1,0:T(8,128)(2,1)} async-done(((bf16[512,512]{1,0:T(8,128)(2,1)}), bf16[512,2048]{1,0:T(8,128)(2,1)}) %all-gather.2.cloned.1.call-update) | async-done | bytes 2097168 | tf_op jit(solution)/shard_map/all_gather | solution.py:34
  61.7 6.6 %fusion.4 = f32[512,1024]{1,0:T(8,128)} fusion(bf16[512,2048]{1,0:T(8,128)(2,1)} %all-gather.2.cloned.1.call-done, bf16[1,2048,1024]{2,1,0:T(8,128)(2,1)} %param.12), kind=kOutput, calls=%fused_computation.5 | convolution fusion | flops 2147483648 | bytes 8388608 | tf_op jit(solution)/shard_map/dot_general | solution.py:35
  68.3 10.0 %fusion.9 = bf16[2048,512]{0,1:T(8,128)(2,1)} fusion(bf16[1,1024,2048]{2,1,0:T(8,128)(2,1)} %param.14, f32[512,1024]{1,0:T(8,128)} %fusion.4, bf16[512,2048]{1,0:T(8,128)(2,1)S(1)} %copy-done.3, bf16[1,2048,1024]{2,1,0:T(8,128)(2,1)} %param.13), kind=kOutput, calls=%fused_computation.8 | convolution fusion | flops 4299161600 | bytes 14680064 | tf_op jit(solution)/shard_map/dot_general | solution.py:40
  78.4 31.3 %reduce-scatter.2.cloned.1.call-done = bf16[512,512]{0,1:T(8,128)(2,1)} async-done(((bf16[2048,512]{0,1:T(8,128)(2,1)}), bf16[512,512]{0,1:T(8,128)(2,1)}) %reduce-scatter.2.cloned.1.call-update) | async-done | bytes 524304 | tf_op jit(solution)/shard_map/reduce_scatter | solution.py:39
  109.7 5.5 %all-to-all-start.1 = ((bf16[512,8,64]{0,2,1:T(8,128)(2,1)}), bf16[512,8,64]{0,2,1:T(8,128)(2,1)S(1)}, u32[]{:S(2)}, u32[]{:S(2)}) async-start(bf16[512,8,64]{0,2,1:T(8,128)(2,1)} %bitcast.45), calls=%async_computation.2 | async-start | bytes 1048576 | tf_op jit(solution)/shard_map/all_to_all | solution.py:47
  115.2 0.1 copy.25
  115.4 0.1 mul.90
  115.5 0.1 copy.24
  115.6 0.1 copy.26
  115.8 13.7 %all-to-all-done.1 = bf16[512,8,64]{0,2,1:T(8,128)(2,1)S(1)} async-done(((bf16[512,8,64]{0,2,1:T(8,128)(2,1)}), bf16[512,8,64]{0,2,1:T(8,128)(2,1)S(1)}, u32[]{:S(2)}, u32[]{:S(2)}) %all-to-all-start.1) | async-done | bytes 524320 | tf_op jit(solution)/shard_map/all_to_all | solution.py:47
  129.5 1.2 gather_fusion
  130.7 0.1 gather.7
  130.8 0.8 multiply_reduce_fusion
  131.7 0.1 multiply_reduce_fusion.1
  131.8 6.0 %psum.15 = f32[128]{0:T(128)S(1)} all-reduce(f32[128]{0:T(128)S(1)} %multiply_reduce_fusion.1), channel_id=1, replica_groups=mesh['ep'=8,'tp'=4] {'tp'}, use_global_device_ids=true, to_apply=%region_9.10 | all-reduce | flops 128 | bytes 1024 | tf_op jit(solution)/shard_map/psum | solution.py:54
  137.7 0.8 fusion.20
  (20 shorter events, 0.1 us)
Async XLA Ops:
  6.5 55.2 %all-gather.2.cloned.1.call-start = ((), (), s32[]{:S(2)}) async-start(), calls=%async_computation.3 | async-start | bytes 2621440 | tf_op jit(solution)/shard_map/all_gather | solution.py:34
  39.9 69.8 %reduce-scatter.2.cloned.1.call-start = ((), (), s32[]{:S(2)}) async-start(), calls=%async_computation.4 | async-start | bytes 2621440 | tf_op jit(solution)/shard_map/reduce_scatter | solution.py:39
  61.7 6.6 %copy-start.3 = (bf16[512,2048]{1,0:T(8,128)(2,1)S(1)}, bf16[512,2048]{1,0:T(8,128)(2,1)}, u32[]{:S(2)}) copy-start(bf16[512,2048]{1,0:T(8,128)(2,1)} %all-gather.2.cloned.1.call-done) | copy-start | bytes 6291460
  78.3 36.9 %copy-start = (s32[128,2]{0,1:T(2,128)S(1)}, s32[128,2]{0,1:T(2,128)}, u32[]{:S(2)}) copy-start(s32[128,2]{0,1:T(2,128)} %param.10) | copy-start | bytes 3076
  78.3 37.3 %copy-start.1 = (f32[128,2]{0,1:T(2,128)S(1)}, f32[128,2]{0,1:T(2,128)}, u32[]{:S(2)}) copy-start(f32[128,2]{0,1:T(2,128)} %param.11) | copy-start | bytes 3076
  78.3 37.4 %copy-start.2 = (bf16[512]{0:T(512)(128)(2,1)S(1)}, bf16[512]{0:T(512)(128)(2,1)}, u32[]{:S(2)}) copy-start(bf16[512]{0:T(512)(128)(2,1)} %param.15) | copy-start | bytes 3076
  109.7 19.8 %all-to-all-start.1 = ((bf16[512,8,64]{0,2,1:T(8,128)(2,1)}), bf16[512,8,64]{0,2,1:T(8,128)(2,1)S(1)}, u32[]{:S(2)}, u32[]{:S(2)}) async-start(bf16[512,8,64]{0,2,1:T(8,128)(2,1)} %bitcast.45), calls=%async_computation.2 | async-start | bytes 1048576 | tf_op jit(solution)/shard_map/all_to_all | solution.py:47
Sparse Core Ops, SparseCore 0:
  40.1 21.6 all-gather.1
  78.5 31.1 reduce-scatter.1
where the time goes:
time: 146 us; the launch traced here: 145 us
  waiting for transfers between devices  66.9 us (46%)
  blocking collectives  33.3 us (23%)
  matrix products  17.9 us (12%)
  between operations  13.5 us (9%)
  starting transfers between devices  5.56 us (4%)
  other arithmetic  4.93 us (3%)
  local copies, waits for them, and re-layouts  3.25 us (2%)
    reduce_scatter x1, waiting for transfers between devices, shards(): lax.psum_scatter(lax.dot_general(down_mat, hidden, (((0,), (1,)), ((), ()...  31.3 us
    all_gather x1, waiting for transfers between devices, shards(): portion = lax.all_gather(arrived, 'tp', axis=1, tiled=True)  21.8 us
    all_to_all x1, blocking collectives, shards(): lax.all_to_all(outgoing, 'ep', split_axis=0, concat_axis=0, tiled=True)  19 us
    all_to_all x1, waiting for transfers between devices, shards(): lax.all_to_all(summed, 'ep', split_axis=1, concat_axis=1, tiled=True)  13.7 us
    dot_general x1, matrix products, shards(): lax.dot_general(down_mat, hidden, (((0,), (1,)), ((), ())), preferred_ele...  10 us
    psum x1, blocking collectives, shards(): row_sums = lax.psum(jnp.sum(x_float * x_float, axis=1), 'tp')  8.37 us
    dot_general x1, matrix products, shards(): gate_sum = jnp.dot(portion, gate_mat, preferred_element_type=jnp.float32)  6.59 us
    psum x1, blocking collectives, shards(): out_sums = lax.psum(jnp.sum(combined * combined, axis=1), 'tp')  5.95 us
  transfers between devices with their start and end apart: 3, of which 3 were waited for; matrix products, arithmetic and copies ran while one was open for 0% of the time, Pallas kernels for 0%

commit v1 on v0

--- a/solution.py
+++ b/solution.py
@@ -26,7 +26,7 @@
     gate_mat = w_gate[0]
     up_mat = w_up[0]
     x_float = tokens.astype(jnp.float32)
-    row_sums = lax.psum(jnp.sum(x_float * x_float, axis=1), "tp")
+    row_sums = jnp.sum(lax.all_gather(jnp.sum(x_float * x_float, axis=1), "tp"), axis=0)
     scale_in = lax.rsqrt(row_sums / full_width + epsilon)
     normed = (x_float * scale_in[:, None] * norm_gain.astype(jnp.float32)).astype(jnp.bfloat16)
     outgoing = jnp.dot(scatter_mat, normed, preferred_element_type=jnp.float32).astype(jnp.bfloat16)

time: 146 us -> 146 us (level)
    psum x1 -> x0, blocking collectives: 8.37 us -> none  [shards(): row_sums = lax.psum(jnp.sum(x_float * x_float, axis=1), 'tp')]
    all_gather x0 -> x1, blocking collectives: none -> 6.01 us  [shards(): lax.all_gather(jnp.sum(x_float * x_float, axis=1), 'tp')]
    all_to_all x1, blocking collectives: 19 us -> 21.3 us  [shards(): lax.all_to_all(outgoing, 'ep', split_axis=0, concat_axis=0, tiled=True)]
where the time goes in v1:
time: 146 us; the launch traced here: 145 us
  waiting for transfers between devices  66.8 us (46%)
  blocking collectives  33.2 us (23%)
  matrix products  17.9 us (12%)
  between operations  13.5 us (9%)
  starting transfers between devices  5.56 us (4%)
  other arithmetic  4.95 us (3%)
  local copies, waits for them, and re-layouts  3.25 us (2%)
    reduce_scatter x1, waiting for transfers between devices, shards(): lax.psum_scatter(lax.dot_general(down_mat, hidden, (((0,), (1,)), ((), ()...  31.3 us
    all_gather x1, waiting for transfers between devices, shards(): portion = lax.all_gather(arrived, 'tp', axis=1, tiled=True)  21.7 us
    all_to_all x1, blocking collectives, shards(): lax.all_to_all(outgoing, 'ep', split_axis=0, concat_axis=0, tiled=True)  21.3 us
    all_to_all x1, waiting for transfers between devices, shards(): lax.all_to_all(summed, 'ep', split_axis=1, concat_axis=1, tiled=True)  13.7 us
    dot_general x1, matrix products, shards(): lax.dot_general(down_mat, hidden, (((0,), (1,)), ((), ())), preferred_ele...  10 us
    dot_general x1, matrix products, shards(): gate_sum = jnp.dot(portion, gate_mat, preferred_element_type=jnp.float32)  6.59 us
    all_gather x1, blocking collectives, shards(): lax.all_gather(jnp.sum(x_float * x_float, axis=1), 'tp')  6.01 us
    psum x1, blocking collectives, shards(): out_sums = lax.psum(jnp.sum(combined * combined, axis=1), 'tp')  5.94 us
  transfers between devices with their start and end apart: 3, of which 3 were waited for; matrix products, arithmetic and copies ran while one was open for 0% of the time, Pallas kernels for 0%

profile of v1, /device:TPU:0, one launch (start us, length us, event | category | flops | bytes accessed | tf_op | source)
XLA Modules:
  0.0 145.2 jit_solution(2727997254043128989)
XLA Ops:
  6.5 0.8 copy.25
  7.3 0.1 eq.39
  7.5 0.1 reshape.81
  7.6 0.6 reduce-window.6
  8.2 0.2 slice_reduce_fusion
  8.5 0.1 fusion.25
  8.6 0.1 reduce_sum.50
  8.7 0.1 copy.27
  8.8 0.7 compare_and_fusion
  9.5 0.1 fusion.16
  9.5 1.0 fusion.17
  10.6 6.0 %all-gather.1 = f32[4,1,128]{2,1,0:T(1,128)S(1)} all-gather(f32[1,1,128]{2,1,0:T(1,128)S(1)} %bitcast.49), channel_id=2, replica_groups=mesh['ep'=8,'tp'=4] {'tp'}, dimensions={0}, use_global_device_ids=true | all-gather | bytes 2560 | tf_op jit(solution)/shard_map/all_gather | solution.py:29
  16.6 0.7 convert_element_type.45
  17.3 1.3 convolution_convert_fusion
  18.6 21.3 %all_to_all.24 = bf16[8,64,512]{2,1,0:T(8,128)(2,1)} all-to-all(bf16[8,64,512]{2,1,0:T(8,128)(2,1)S(1)} %bitcast.44), channel_id=1, replica_groups=mesh['ep'=8,'tp'=4] {'ep'}, dimensions={0} | all-to-all | bytes 1048576 | tf_op jit(solution)/shard_map/all_to_all | solution.py:33
  39.8 0.0 reduce-scatter.2.cloned.1.call-start
  39.9 21.7 %all-gather.4.cloned.1.call-done = bf16[512,2048]{1,0:T(8,128)(2,1)} async-done(((bf16[512,512]{1,0:T(8,128)(2,1)}), bf16[512,2048]{1,0:T(8,128)(2,1)}) %all-gather.4.cloned.1.call-update) | async-done | bytes 2097168 | tf_op jit(solution)/shard_map/all_gather | solution.py:34
  61.6 6.6 %fusion.4 = f32[512,1024]{1,0:T(8,128)} fusion(bf16[512,2048]{1,0:T(8,128)(2,1)} %all-gather.4.cloned.1.call-done, bf16[1,2048,1024]{2,1,0:T(8,128)(2,1)} %param.12), kind=kOutput, calls=%fused_computation.5 | convolution fusion | flops 2147483648 | bytes 8388608 | tf_op jit(solution)/shard_map/dot_general | solution.py:35
  68.2 10.0 %fusion.9 = bf16[2048,512]{0,1:T(8,128)(2,1)} fusion(bf16[1,1024,2048]{2,1,0:T(8,128)(2,1)} %param.14, f32[512,1024]{1,0:T(8,128)} %fusion.4, bf16[512,2048]{1,0:T(8,128)(2,1)S(1)} %copy-done.3, bf16[1,2048,1024]{2,1,0:T(8,128)(2,1)} %param.13), kind=kOutput, calls=%fused_computation.8 | convolution fusion | flops 4299161600 | bytes 14680064 | tf_op jit(solution)/shard_map/dot_general | solution.py:40
  78.2 31.3 %reduce-scatter.2.cloned.1.call-done = bf16[512,512]{0,1:T(8,128)(2,1)} async-done(((bf16[2048,512]{0,1:T(8,128)(2,1)}), bf16[512,512]{0,1:T(8,128)(2,1)}) %reduce-scatter.2.cloned.1.call-update) | async-done | bytes 524304 | tf_op jit(solution)/shard_map/reduce_scatter | solution.py:39
  109.6 5.5 %all-to-all-start.1 = ((bf16[512,8,64]{0,2,1:T(8,128)(2,1)}), bf16[512,8,64]{0,2,1:T(8,128)(2,1)S(1)}, u32[]{:S(2)}, u32[]{:S(2)}) async-start(bf16[512,8,64]{0,2,1:T(8,128)(2,1)} %bitcast.46), calls=%async_computation.2 | async-start | bytes 1048576 | tf_op jit(solution)/shard_map/all_to_all | solution.py:47
  115.1 0.1 copy.29
  115.2 0.1 mul.90
  115.4 0.1 copy.28
  115.5 0.1 copy.30
  115.7 13.7 %all-to-all-done.1 = bf16[512,8,64]{0,2,1:T(8,128)(2,1)S(1)} async-done(((bf16[512,8,64]{0,2,1:T(8,128)(2,1)}), bf16[512,8,64]{0,2,1:T(8,128)(2,1)S(1)}, u32[]{:S(2)}, u32[]{:S(2)}) %all-to-all-start.1) | async-done | bytes 524320 | tf_op jit(solution)/shard_map/all_to_all | solution.py:47
  129.4 1.2 gather_fusion
  130.6 0.1 gather.7
  130.7 0.8 multiply_reduce_fusion
  131.5 0.1 multiply_reduce_fusion.1
  131.6 5.9 %psum.7 = f32[128]{0:T(128)S(1)} all-reduce(f32[128]{0:T(128)S(1)} %multiply_reduce_fusion.1), channel_id=1, replica_groups=mesh['ep'=8,'tp'=4] {'tp'}, use_global_device_ids=true, to_apply=%region_9.10 | all-reduce | flops 128 | bytes 1024 | tf_op jit(solution)/shard_map/psum | solution.py:54
  137.6 0.8 fusion.20
  (21 shorter events, 0.2 us)
Async XLA Ops:
  6.5 55.1 %all-gather.4.cloned.1.call-start = ((), (), s32[]{:S(2)}) async-start(), calls=%async_computation.3 | async-start | bytes 2621440 | tf_op jit(solution)/shard_map/all_gather | solution.py:34
  39.8 69.7 %reduce-scatter.2.cloned.1.call-start = ((), (), s32[]{:S(2)}) async-start(), calls=%async_computation.4 | async-start | bytes 2621440 | tf_op jit(solution)/shard_map/reduce_scatter | solution.py:39
  61.6 6.6 %copy-start.3 = (bf16[512,2048]{1,0:T(8,128)(2,1)S(1)}, bf16[512,2048]{1,0:T(8,128)(2,1)}, u32[]{:S(2)}) copy-start(bf16[512,2048]{1,0:T(8,128)(2,1)} %all-gather.4.cloned.1.call-done) | copy-start | bytes 6291460
  78.2 36.9 %copy-start = (s32[128,2]{0,1:T(2,128)S(1)}, s32[128,2]{0,1:T(2,128)}, u32[]{:S(2)}) copy-start(s32[128,2]{0,1:T(2,128)} %param.10) | copy-start | bytes 3076
  78.2 37.3 %copy-start.1 = (f32[128,2]{0,1:T(2,128)S(1)}, f32[128,2]{0,1:T(2,128)}, u32[]{:S(2)}) copy-start(f32[128,2]{0,1:T(2,128)} %param.11) | copy-start | bytes 3076
  78.2 37.4 %copy-start.2 = (bf16[512]{0:T(512)(128)(2,1)S(1)}, bf16[512]{0:T(512)(128)(2,1)}, u32[]{:S(2)}) copy-start(bf16[512]{0:T(512)(128)(2,1)} %param.15) | copy-start | bytes 3076
  109.6 19.8 %all-to-all-start.1 = ((bf16[512,8,64]{0,2,1:T(8,128)(2,1)}), bf16[512,8,64]{0,2,1:T(8,128)(2,1)S(1)}, u32[]{:S(2)}, u32[]{:S(2)}) async-start(bf16[512,8,64]{0,2,1:T(8,128)(2,1)} %bitcast.46), calls=%async_computation.2 | async-start | bytes 1048576 | tf_op jit(solution)/shard_map/all_to_all | solution.py:47
Sparse Core Ops, SparseCore 0:
  40.0 21.5 all-gather.3
  78.4 31.1 reduce-scatter.1
